TPU v7x, 32 devices: a whole 2x2x4 slice. The times are simulated.
32 devices in a mesh: kv: 16 (over z, x, core), tp: 2 (over y).
Axes of the slice: x: 2, y: 2, z: 4, core: 2. Of those that a mesh axis runs over, the one named last changes fastest.
Arguments:
- hidden_in: bfloat16 [4, 1024, 2048], P(None, 'kv'), may hold values from -84 to 84
- w_query: bfloat16 [2048, 1024], P(None, 'tp'), may hold values from -0.125 to 0.125
- w_cmp_key: bfloat16 [2048, 256], P(None, 'tp'), may hold values from -0.125 to 0.125
- w_cmp_value: bfloat16 [2048, 256], P(None, 'tp'), may hold values from -0.8838835 to 0.8838835
- w_sel_key: bfloat16 [2048, 256], P(None, 'tp'), may hold values from -0.125 to 0.125
- w_sel_value: bfloat16 [2048, 256], P(None, 'tp'), may hold values from -0.8838835 to 0.8838835
- w_gate: bfloat16 [2048, 2, 16], replicated, may hold values from -0.125 to 0.125
- cmp_key_in: bfloat16 [2048, 128], replicated, may hold values from -0.125 to 0.125
- cmp_key_out: bfloat16 [128, 64], replicated, may hold values from -0.5 to 0.5
- cmp_value_in: bfloat16 [2048, 128], replicated, may hold values from -0.125 to 0.125
- cmp_value_out: bfloat16 [128, 64], replicated, may hold values from -0.5 to 0.5
- out_gain: float32 [1024], replicated, may hold values from 0.1 to 1.9
- w_out: bfloat16 [1024, 2048], replicated, may hold values from -0.1875 to 0.1875
- seq_lengths: int32 [4], replicated, may hold values from 1 to 1024, 1638 in all
- chosen: int32 [4, 16, 4, 16], P(None, 'kv', 'tp'), may hold values from -1 to 15, as said below
Outputs:
- attended: bfloat16 [4, 1024, 2048], P(None, 'kv', 'tp')
Inputs may be any that keep to these rules, and one draw needn't show every extreme that they name: chosen[s, b, g, 0] is b itself. Every other entry is -1 or a block index below b, and the entries of one list that are not -1 are distinct. For each block index and key group, the entries after the first slot that name that index all lie in the lists of a single sequence.
All inputs are finite; a program needn't handle non-finite values.
Results may differ from a plain program's by a relative error of at most 0.012.
The roundings to bfloat16 on the way count: a program that leaves them out, or rounds other values in their place, can miss the bound.
Values may be sent and summed in bfloat16 or wider, within the bound.
A program may use at most 64 MiB of HBM per device.

v0:
```python
import jax
import jax.numpy as jnp
from jax import lax
from jax.sharding import PartitionSpec as P

HEADS = 16
HEAD_DIM = 64
CMP_STRIDE = 16
CMP_BLOCK = 32
TOPK = 16
theta_base = 500000.0
norm_eps = 1e-06


def rotate(values, positions):
    width = values.shape[-1]
    half = width // 2
    inverse = jnp.exp(
        -jnp.log(jnp.float32(theta_base)) * jnp.arange(0, width, 2).astype(jnp.float32) / width
    )
    angle = positions.astype(jnp.float32)[:, None] * inverse[None, :]
    cosine = jnp.cos(angle)[:, None, :]
    sine = jnp.sin(angle)[:, None, :]
    first = values[..., :half]
    second = values[..., half:]
    return jnp.concatenate(
        [first * cosine - second * sine, second * cosine + first * sine], axis=-1
    )


def masked_weights(scores, valid):
    top = jnp.max(jnp.where(valid, scores, -1e30), axis=-1, keepdims=True)
    expd = jnp.where(valid, jnp.exp(scores - top), 0.0)
    total = jnp.sum(expd, axis=-1, keepdims=True)
    return (expd / jnp.maximum(total, 1.0)).astype(jnp.bfloat16)


def compress(raw, prior, weight_in, weight_out):
    seqs, span, groups, width = raw.shape
    extended = jnp.concatenate([prior, raw], axis=1)
    count = span // CMP_STRIDE
    front = extended[:, :span].reshape(seqs, count, CMP_STRIDE, groups, width)
    back = extended[:, CMP_STRIDE:].reshape(seqs, count, CMP_STRIDE, groups, width)
    window = jnp.concatenate([front, back], axis=2).transpose(0, 1, 3, 2, 4)
    window = window.reshape(seqs * count * groups, CMP_BLOCK * width)
    inner = jax.nn.gelu(jnp.dot(window, weight_in, preferred_element_type=jnp.float32)).astype(
        jnp.bfloat16
    )
    return jnp.dot(inner, weight_out, preferred_element_type=jnp.float32).reshape(
        seqs, count, groups, width
    )


def shards(
    hidden_in,
    w_query,
    w_cmp_key,
    w_cmp_value,
    w_sel_key,
    w_sel_value,
    w_gate,
    cmp_key_in,
    cmp_key_out,
    cmp_value_in,
    cmp_value_out,
    out_gain,
    w_out,
    seq_lengths,
    chosen,
):
    seqs, span, width = hidden_in.shape
    block_list = lax.axis_size("kv")
    place = lax.axis_index("kv")
    column = lax.axis_index("tp")
    local_heads = w_query.shape[1] // HEAD_DIM
    local_groups = w_sel_key.shape[1] // HEAD_DIM
    per_group = local_heads // local_groups
    count = span // CMP_STRIDE
    scale = HEAD_DIM ** (-0.5)
    rows = hidden_in.reshape(seqs * span, width)
    positions = place * span + jnp.arange(span, dtype=jnp.int32)

    def project(weight_matrix, heads):
        return jnp.dot(rows, weight_matrix, preferred_element_type=jnp.float32).reshape(
            seqs, span, heads, HEAD_DIM
        )

    queries = rotate(project(w_query, local_heads), positions).astype(jnp.bfloat16)
    sel_pairs = jnp.concatenate(
        [rotate(project(w_sel_key, local_groups), positions), project(w_sel_value, local_groups)],
        axis=-1,
    ).astype(jnp.bfloat16)
    raw_pairs = jnp.concatenate(
        [project(w_cmp_key, local_groups), project(w_cmp_value, local_groups)], axis=-1
    ).astype(jnp.bfloat16)
    prior = jnp.zeros((seqs, CMP_STRIDE, local_groups, HEAD_DIM), jnp.bfloat16)
    ends = place * span + jnp.arange(count, dtype=jnp.int32) * CMP_STRIDE + CMP_STRIDE - 1
    cmp_keys = rotate(compress(raw_pairs[..., :HEAD_DIM], prior, cmp_key_in, cmp_key_out), ends)
    cmp_values = compress(raw_pairs[..., HEAD_DIM:], prior, cmp_value_in, cmp_value_out)
    cmp_piece = jnp.concatenate(
        [cmp_keys.astype(jnp.bfloat16), cmp_values.astype(jnp.bfloat16)], axis=-1
    )[:, None]
    picks = chosen[:, 0]
    every_list = lax.all_gather(picks[None, :, :, 1:], "kv", axis=0, tiled=True)
    named = jnp.any(every_list == place, axis=(0, 3)).astype(jnp.int32)
    seq_ids = jnp.arange(seqs, dtype=jnp.int32)[:, None]
    exported_seq = jnp.sum(named * seq_ids, axis=0)
    selector = seq_ids == exported_seq[None, :]
    export = jnp.sum(
        jnp.where(selector[:, None, :, None], sel_pairs, jnp.zeros((), jnp.bfloat16)), axis=0
    )
    export = export[None]
    remote_pairs, remote_entries = (
        lax.all_gather(export, "kv", axis=0, tiled=True),
        lax.all_gather(cmp_piece, "kv", axis=1, tiled=True),
    )
    gate_all = jnp.dot(rows, w_gate.reshape(width, 2 * HEADS), preferred_element_type=jnp.float32)
    gate_all = gate_all.reshape(seqs, span, 2, HEADS)
    gates = jax.nn.sigmoid(lax.dynamic_slice_in_dim(gate_all, column * local_heads, local_heads, 3))
    entry = jnp.arange(block_list * count, dtype=jnp.int32)
    entry_end = entry * CMP_STRIDE + CMP_STRIDE - 1
    cmp_valid = ((entry >= 1)[None, :] & (entry_end[None, :] <= positions[:, None]))[None, None]
    key_pos = jnp.arange(span, dtype=jnp.int32)
    own_valid = key_pos[None, :] <= key_pos[:, None]

    def one_sequence(args):
        seq_queries, seq_entries, seq_picks, seq_pairs, seq_gates, seq_length = args
        block_q = seq_queries.reshape(span, local_groups, per_group, HEAD_DIM)
        entries = seq_entries.reshape(block_list * count, local_groups, 2 * HEAD_DIM)
        scores = (
            jnp.einsum(
                "qghd,egd->ghqe",
                block_q,
                entries[..., :HEAD_DIM],
                preferred_element_type=jnp.float32,
            )
            * scale
        )
        weights = masked_weights(scores, cmp_valid)
        cmp_out = jnp.einsum(
            "ghqe,egd->qghd", weights, entries[..., HEAD_DIM:], preferred_element_type=jnp.float32
        )
        far = jnp.maximum(seq_picks[:, 1:], 0)
        fetched = jax.vmap(lambda table, index: table[index], in_axes=(2, 0))(remote_pairs, far)
        near = jnp.transpose(seq_pairs, (1, 0, 2))[:, None]
        pairs = jnp.concatenate([near, fetched], axis=1).reshape(
            local_groups, TOPK * span, 2 * HEAD_DIM
        )
        far_live = jnp.broadcast_to(
            (seq_picks[:, 1:] >= 0)[:, None, :, None], (local_groups, span, TOPK - 1, span)
        )
        near_live = jnp.broadcast_to(own_valid[None, :, None, :], (local_groups, span, 1, span))
        sel_valid = jnp.concatenate([near_live, far_live], axis=2).reshape(
            local_groups, 1, span, TOPK * span
        )
        scores_s = (
            jnp.einsum(
                "qghd,gmd->ghqm", block_q, pairs[..., :HEAD_DIM], preferred_element_type=jnp.float32
            )
            * scale
        )
        weights_s = masked_weights(scores_s, sel_valid)
        sel_out = jnp.einsum(
            "ghqm,gmd->qghd", weights_s, pairs[..., HEAD_DIM:], preferred_element_type=jnp.float32
        )
        split = seq_gates.reshape(span, 2, local_groups, per_group, 1)
        mixed = split[:, 0] * cmp_out + split[:, 1] * sel_out
        mixed = jnp.where((positions < seq_length)[:, None, None, None], mixed, 0.0)
        return mixed.reshape(span, local_heads * HEAD_DIM).astype(jnp.bfloat16)

    mixed = lax.map(one_sequence, (queries, remote_entries, picks, sel_pairs, gates, seq_lengths))
    mixed = mixed.reshape(seqs * span, local_heads * HEAD_DIM)
    out_width = width // lax.axis_size("tp")
    own_columns = lax.dynamic_slice_in_dim(w_out, column * out_width, out_width, 1)
    piece_wide = lax.all_gather(mixed, "tp", axis=1, tiled=True).astype(jnp.float32)
    scaled_piece = (piece_wide * out_gain[None, :]).astype(jnp.bfloat16)
    total = jnp.dot(scaled_piece, own_columns, preferred_element_type=jnp.float32)
    squares = jnp.sum(piece_wide * piece_wide, axis=-1)
    row_scale = lax.rsqrt(squares / (HEADS * HEAD_DIM) + norm_eps)
    return (total * row_scale[:, None]).astype(jnp.bfloat16).reshape(seqs, span, out_width)


def solution(mesh):
    placed = (
        P(None, "kv", None),
        P(None, "tp"),
        P(None, "tp"),
        P(None, "tp"),
        P(None, "tp"),
        P(None, "tp"),
        P(),
        P(),
        P(),
        P(),
        P(),
        P(),
        P(),
        P(),
        P(None, "kv", "tp", None),
    )
    return jax.shard_map(
        shards, mesh=mesh, in_specs=placed, out_specs=P(None, "kv", "tp"), check_vma=False
    )
```

profile of v0, /device:TPU:0, one launch (start us, length us, event | category | flops | bytes accessed | tf_op | source)
XLA Modules:
  0.0 139.8 jit_solution(10767838875273096668)
XLA Ops:
  0.2 1.3 copy.65
  2.6 23.3 %all-gather.1 = s32[64,2,15]{2,1,0:T(2,128)S(1)} all-gather(s32[4,2,15]{2,1,0:T(2,128)S(1)} %slice.87), channel_id=3, replica_groups=mesh['kv'=16,'tp'=2] {'kv'}, dimensions={0}, use_global_device_ids=true | all-gather | bytes 8160 | tf_op jit(solution)/shard_map/all_gather | solution.py:104
  25.9 1.2 compare_reduce_fusion
  28.2 18.9 %all-gather.2 = bf16[1024,2,128]{2,0,1:T(8,128)(2,1)S(1)} all-gather(bf16[64,2,128]{2,0,1:T(8,128)(2,1)S(1)} %get-tuple-element.167), channel_id=4, replica_groups=mesh['kv'=16,'tp'=2] {'kv'}, dimensions={0}, use_global_device_ids=true | all-gather | bytes 557056 | tf_op jit(solution)/shard_map/all_gather | solution.py:114
  47.2 1.0 copy.55
  48.2 1.8 %convolution_convert_fusion.2 = bf16[4,64,2,64]{1,3,2,0:T(8,128)(2,1)S(1)} fusion(bf16[2,64,2048,1]{2,1,0,3:T(8,128)(2,1)} %bitcast.227, bf16[4,64,2048]{2,1,0:T(8,128)(2,1)S(1)} %copy-done), kind=kOutput, calls=%fused_computation.71 | convolution fusion | flops 134250496 | bytes 1638400 | tf_op jit(solution)/shard_map/dot_general | solution.py:84
  51.1 1.2 copy.59
  54.3 19.1 %all-gather = bf16[4,64,2,128]{3,2,1,0:T(2,128)(2,1)S(1)} all-gather(bf16[4,4,2,128]{3,2,1,0:T(2,128)(2,1)S(1)} %pad_maximum_fusion.3), channel_id=2, replica_groups=mesh['kv'=16,'tp'=2] {'kv'}, dimensions={1}, use_global_device_ids=true | all-gather | bytes 139264 | tf_op jit(solution)/shard_map/all_gather | solution.py:115
  74.1 4.0 %copy.64 = bf16[2048,512]{0,1:T(8,128)(2,1)} copy(bf16[2048,512]{1,0:T(8,128)(2,1)} %param.18) | data formatting | bytes 4194304 | tf_op args[1]
  78.1 2.8 %fusion.54 = f32[4,64,8,64]{1,3,2,0:T(8,128)S(1)} fusion(bf16[8,64,2048,1]{2,1,0,3:T(8,128)(2,1)} %bitcast.222, bf16[4,64,2048]{2,1,0:T(8,128)(2,1)S(1)} %copy-done), kind=kOutput, calls=%fused_computation.78 | convolution fusion | flops 536870912 | bytes 3670016 | tf_op jit(solution)/shard_map/dot_general | solution.py:84
  83.1 43.9 %while.11 = (s32[]{:T(128)}, bf16[4,64,512]{2,1,0:T(8,128)(2,1)}, s32[4]{0:T(128)}, f32[4,64,2,8]{1,3,2,0:T(8,128)}, bf16[4,16,4,2,128]{4,2,1,3,0:T(4,128)(2,1)}...) while((s32[]{:T(128)}, bf16[4,64,512]{2,1,0:T(8,128)(2,1)}, ...), condition=%wide.region_8.9_spmd.clone, body=%wide.region_3.8_spmd.clone.sunk | while | flops 147700704 | bytes 25832684 | solution.py:171
  84.2 0.7 copy-done.1
  86.0 1.1 broadcast_in_dim.207
  87.1 1.8 %fusion.134 = (f32[2,4,64]{2,1,0:T(4,128)S(1)}, f32[2,4,64,1024]{3,2,1,0:T(8,128)S(1)}) fusion(f32[2,1024,64,4]{1,2,3,0:T(8,128)S(1)} %fusion.133, pred[2,64,1024]{2,1,0:T(8,128)(4,1)} %broadcast_in_dim.207), kind=kOutput, calls=%fused_computation.151.clone.1 | output fusion | flops 3146751 | bytes 4327424 | tf_op jit(solution)/shard_map/while/body/eval_jaxpr/sub | solution.py:33
  89.6 0.9 fusion.135
  90.5 0.9 constant_dynamic-slice_fusion.9
  95.2 0.7 copy-done.1
  97.0 1.1 broadcast_in_dim.207
  98.0 1.8 %fusion.134 = (f32[2,4,64]{2,1,0:T(4,128)S(1)}, f32[2,4,64,1024]{3,2,1,0:T(8,128)S(1)}) fusion(f32[2,1024,64,4]{1,2,3,0:T(8,128)S(1)} %fusion.133, pred[2,64,1024]{2,1,0:T(8,128)(4,1)} %broadcast_in_dim.207), kind=kOutput, calls=%fused_computation.151.clone.1 | output fusion | flops 3146751 | bytes 4327424 | tf_op jit(solution)/shard_map/while/body/eval_jaxpr/sub | solution.py:33
  100.6 0.9 fusion.135
  101.5 0.9 constant_dynamic-slice_fusion.9
  106.2 0.7 copy-done.1
  107.9 1.1 broadcast_in_dim.207
  109.0 1.8 %fusion.134 = (f32[2,4,64]{2,1,0:T(4,128)S(1)}, f32[2,4,64,1024]{3,2,1,0:T(8,128)S(1)}) fusion(f32[2,1024,64,4]{1,2,3,0:T(8,128)S(1)} %fusion.133, pred[2,64,1024]{2,1,0:T(8,128)(4,1)} %broadcast_in_dim.207), kind=kOutput, calls=%fused_computation.151.clone.1 | output fusion | flops 3146751 | bytes 4327424 | tf_op jit(solution)/shard_map/while/body/eval_jaxpr/sub | solution.py:33
  111.5 0.9 fusion.135
  112.5 0.9 constant_dynamic-slice_fusion.9
  118.9 1.1 broadcast_in_dim.207
  120.0 1.8 %fusion.134 = (f32[2,4,64]{2,1,0:T(4,128)S(1)}, f32[2,4,64,1024]{3,2,1,0:T(8,128)S(1)}) fusion(f32[2,1024,64,4]{1,2,3,0:T(8,128)S(1)} %fusion.133, pred[2,64,1024]{2,1,0:T(8,128)(4,1)} %broadcast_in_dim.207), kind=kOutput, calls=%fused_computation.151.clone.1 | output fusion | flops 3146751 | bytes 4327424 | tf_op jit(solution)/shard_map/while/body/eval_jaxpr/sub | solution.py:33
  122.5 0.9 fusion.135
  123.5 0.9 constant_dynamic-slice_fusion.9
  127.0 9.4 %all_gather.15 = bf16[256,1024]{1,0:T(8,128)(2,1)S(1)} all-gather(bf16[256,512]{1,0:T(8,128)(2,1)} %bitcast.233), channel_id=1, replica_groups=mesh['kv'=16,'tp'=2] {'tp'}, dimensions={1}, use_global_device_ids=true | all-gather | bytes 786432 | tf_op jit(solution)/shard_map/all_gather | solution.py:175
  136.7 3.1 %fusion.46 = bf16[256,1024]{1,0:T(8,128)(2,1)} fusion(bf16[1024,2048]{1,0:T(8,128)(2,1)} %param.29, s32[]{:T(128)S(6)} %select_n.31, bf16[256,1024]{1,0:T(8,128)(2,1)S(1)} %all_gather.15, f32[256]{0:T(256)S(1)} %add_rsqrt_fusion, f32[1024]{0:T(1024)} %param.28), kind=kOutput, calls=%fused_computation.68 | convolution fusion | flops 538181632 | bytes 3150852 | tf_op jit(solution)/shard_map/dot_general | solution.py:177
  (231 shorter events, 30.6 us)
Async XLA Ops:
  0.0 1.5 %copy-start = (bf16[4,64,2048]{2,1,0:T(8,128)(2,1)S(1)}, bf16[4,64,2048]{2,1,0:T(8,128)(2,1)}, u32[]{:S(2)}) copy-start(bf16[4,64,2048]{2,1,0:T(8,128)(2,1)} %param.17) | copy-start | bytes 3145732
  0.0 2.5 %copy-start.14 = (s32[4,1,2,16]{3,2,1,0:T(2,128)S(1)}, s32[4,1,2,16]{3,2,1,0:T(2,128)}, u32[]{:S(2)}) copy-start(s32[4,1,2,16]{3,2,1,0:T(2,128)} %param.31) | copy-start | bytes 1540
  0.0 27.3 %copy-start.9 = (bf16[2048,128]{1,0:T(8,128)(2,1)S(1)}, bf16[2048,128]{1,0:T(8,128)(2,1)}, u32[]{:S(2)}) copy-start(bf16[2048,128]{1,0:T(8,128)(2,1)} %param.22) | copy-start | bytes 1572868
  25.9 21.3 %copy-start.10 = (bf16[2048,128]{1,0:T(8,128)(2,1)S(1)}, bf16[2048,128]{1,0:T(8,128)(2,1)}, u32[]{:S(2)}) copy-start(bf16[2048,128]{1,0:T(8,128)(2,1)} %param.19) | copy-start | bytes 1572868
  48.2 2.5 %copy-start.11 = (bf16[2048,128]{1,0:T(8,128)(2,1)S(1)}, bf16[2048,128]{1,0:T(8,128)(2,1)}, u32[]{:S(2)}) copy-start(bf16[2048,128]{1,0:T(8,128)(2,1)} %param.24) | copy-start | bytes 1572868
  48.2 2.5 %copy-start.15 = (bf16[128,64]{0,1:T(8,128)(2,1)S(1)}, bf16[128,64]{0,1:T(8,128)(2,1)}, u32[]{:S(2)}) copy-start(bf16[128,64]{0,1:T(8,128)(2,1)} %param.25) | copy-start | bytes 49156
  52.4 1.5 %copy-start.12 = (bf16[2048,128]{1,0:T(8,128)(2,1)S(1)}, bf16[2048,128]{1,0:T(8,128)(2,1)}, u32[]{:S(2)}) copy-start(bf16[2048,128]{1,0:T(8,128)(2,1)} %param.26) | copy-start | bytes 1572868
  52.4 1.5 %copy-start.16 = (bf16[128,64]{0,1:T(8,128)(2,1)S(1)}, bf16[128,64]{0,1:T(8,128)(2,1)}, u32[]{:S(2)}) copy-start(bf16[128,64]{0,1:T(8,128)(2,1)} %param.27) | copy-start | bytes 49156
  83.1 1.1 copy-start.3
  83.1 1.1 copy-start.5
  83.1 1.1 copy-start.7
  87.1 2.5 %copy-start.2 = (bf16[2,16,64,128]{3,2,1,0:T(8,128)(2,1)S(1)}, bf16[2,16,64,128]{3,2,1,0:T(8,128)(2,1)}, u32[]{:S(2)}) copy-start(bf16[2,16,64,128]{3,2,1,0:T(8,128)(2,1)} %copy-done.1) | copy-start | bytes 1572868 | tf_op jit(solution)/shard_map/while
  89.6 2.2 %copy-start.17 = (s32[4]{0:T(128)S(1)}, s32[4]{0:T(128)}, u32[]{:S(2)}) copy-start(s32[4]{0:T(128)} %get-tuple-element.302) | copy-start | bytes 52 | tf_op jit(solution)/shard_map/while
  90.5 3.6 %copy-start.4 = (bf16[16,64,2,128]{3,1,0,2:T(8,128)(2,1)S(1)}, bf16[16,64,2,128]{3,1,0,2:T(8,128)(2,1)}, u32[]{:S(2)}) copy-start(bf16[16,64,2,128]{3,1,0,2:T(8,128)(2,1)} %copy-done.3) | copy-start | bytes 1572868 | tf_op jit(solution)/shard_map/while
  90.5 3.6 %copy-start.6 = (bf16[4,64,8,64]{1,3,2,0:T(8,128)(2,1)S(1)}, bf16[4,64,8,64]{1,3,2,0:T(8,128)(2,1)}, u32[]{:S(2)}) copy-start(bf16[4,64,8,64]{1,3,2,0:T(8,128)(2,1)} %copy-done.5) | copy-start | bytes 786436 | tf_op jit(solution)/shard_map/while
  90.5 3.6 %copy-start.8 = (bf16[4,64,2,128]{3,1,2,0:T(8,128)(2,1)S(1)}, bf16[4,64,2,128]{3,1,2,0:T(8,128)(2,1)}, u32[]{:S(2)}) copy-start(bf16[4,64,2,128]{3,1,2,0:T(8,128)(2,1)} %copy-done.7) | copy-start | bytes 393220 | tf_op jit(solution)/shard_map/while
  94.1 1.1 copy-start.5
  98.0 2.5 %copy-start.2 = (bf16[2,16,64,128]{3,2,1,0:T(8,128)(2,1)S(1)}, bf16[2,16,64,128]{3,2,1,0:T(8,128)(2,1)}, u32[]{:S(2)}) copy-start(bf16[2,16,64,128]{3,2,1,0:T(8,128)(2,1)} %copy-done.1) | copy-start | bytes 1572868 | tf_op jit(solution)/shard_map/while
  100.6 2.2 %copy-start.17 = (s32[4]{0:T(128)S(1)}, s32[4]{0:T(128)}, u32[]{:S(2)}) copy-start(s32[4]{0:T(128)} %get-tuple-element.302) | copy-start | bytes 52 | tf_op jit(solution)/shard_map/while
  101.5 3.6 %copy-start.4 = (bf16[16,64,2,128]{3,1,0,2:T(8,128)(2,1)S(1)}, bf16[16,64,2,128]{3,1,0,2:T(8,128)(2,1)}, u32[]{:S(2)}) copy-start(bf16[16,64,2,128]{3,1,0,2:T(8,128)(2,1)} %copy-done.3) | copy-start | bytes 1572868 | tf_op jit(solution)/shard_map/while
  101.5 3.6 %copy-start.6 = (bf16[4,64,8,64]{1,3,2,0:T(8,128)(2,1)S(1)}, bf16[4,64,8,64]{1,3,2,0:T(8,128)(2,1)}, u32[]{:S(2)}) copy-start(bf16[4,64,8,64]{1,3,2,0:T(8,128)(2,1)} %copy-done.5) | copy-start | bytes 786436 | tf_op jit(solution)/shard_map/while
  101.5 3.6 %copy-start.8 = (bf16[4,64,2,128]{3,1,2,0:T(8,128)(2,1)S(1)}, bf16[4,64,2,128]{3,1,2,0:T(8,128)(2,1)}, u32[]{:S(2)}) copy-start(bf16[4,64,2,128]{3,1,2,0:T(8,128)(2,1)} %copy-done.7) | copy-start | bytes 393220 | tf_op jit(solution)/shard_map/while
  109.0 2.5 %copy-start.2 = (bf16[2,16,64,128]{3,2,1,0:T(8,128)(2,1)S(1)}, bf16[2,16,64,128]{3,2,1,0:T(8,128)(2,1)}, u32[]{:S(2)}) copy-start(bf16[2,16,64,128]{3,2,1,0:T(8,128)(2,1)} %copy-done.1) | copy-start | bytes 1572868 | tf_op jit(solution)/shard_map/while
  111.5 2.2 %copy-start.17 = (s32[4]{0:T(128)S(1)}, s32[4]{0:T(128)}, u32[]{:S(2)}) copy-start(s32[4]{0:T(128)} %get-tuple-element.302) | copy-start | bytes 52 | tf_op jit(solution)/shard_map/while
  112.5 3.6 %copy-start.4 = (bf16[16,64,2,128]{3,1,0,2:T(8,128)(2,1)S(1)}, bf16[16,64,2,128]{3,1,0,2:T(8,128)(2,1)}, u32[]{:S(2)}) copy-start(bf16[16,64,2,128]{3,1,0,2:T(8,128)(2,1)} %copy-done.3) | copy-start | bytes 1572868 | tf_op jit(solution)/shard_map/while
  112.5 3.6 %copy-start.6 = (bf16[4,64,8,64]{1,3,2,0:T(8,128)(2,1)S(1)}, bf16[4,64,8,64]{1,3,2,0:T(8,128)(2,1)}, u32[]{:S(2)}) copy-start(bf16[4,64,8,64]{1,3,2,0:T(8,128)(2,1)} %copy-done.5) | copy-start | bytes 786436 | tf_op jit(solution)/shard_map/while
  112.5 3.6 %copy-start.8 = (bf16[4,64,2,128]{3,1,2,0:T(8,128)(2,1)S(1)}, bf16[4,64,2,128]{3,1,2,0:T(8,128)(2,1)}, u32[]{:S(2)}) copy-start(bf16[4,64,2,128]{3,1,2,0:T(8,128)(2,1)} %copy-done.7) | copy-start | bytes 393220 | tf_op jit(solution)/shard_map/while
  120.0 2.5 %copy-start.2 = (bf16[2,16,64,128]{3,2,1,0:T(8,128)(2,1)S(1)}, bf16[2,16,64,128]{3,2,1,0:T(8,128)(2,1)}, u32[]{:S(2)}) copy-start(bf16[2,16,64,128]{3,2,1,0:T(8,128)(2,1)} %copy-done.1) | copy-start | bytes 1572868 | tf_op jit(solution)/shard_map/while
  122.5 2.2 %copy-start.17 = (s32[4]{0:T(128)S(1)}, s32[4]{0:T(128)}, u32[]{:S(2)}) copy-start(s32[4]{0:T(128)} %get-tuple-element.302) | copy-start | bytes 52 | tf_op jit(solution)/shard_map/while
  123.5 3.6 %copy-start.4 = (bf16[16,64,2,128]{3,1,0,2:T(8,128)(2,1)S(1)}, bf16[16,64,2,128]{3,1,0,2:T(8,128)(2,1)}, u32[]{:S(2)}) copy-start(bf16[16,64,2,128]{3,1,0,2:T(8,128)(2,1)} %copy-done.3) | copy-start | bytes 1572868 | tf_op jit(solution)/shard_map/while
  123.5 3.6 %copy-start.6 = (bf16[4,64,8,64]{1,3,2,0:T(8,128)(2,1)S(1)}, bf16[4,64,8,64]{1,3,2,0:T(8,128)(2,1)}, u32[]{:S(2)}) copy-start(bf16[4,64,8,64]{1,3,2,0:T(8,128)(2,1)} %copy-done.5) | copy-start | bytes 786436 | tf_op jit(solution)/shard_map/while
  123.5 3.6 %copy-start.8 = (bf16[4,64,2,128]{3,1,2,0:T(8,128)(2,1)S(1)}, bf16[4,64,2,128]{3,1,2,0:T(8,128)(2,1)}, u32[]{:S(2)}) copy-start(bf16[4,64,2,128]{3,1,2,0:T(8,128)(2,1)} %copy-done.7) | copy-start | bytes 393220 | tf_op jit(solution)/shard_map/while
  (13 other events, 12.5 us)
where the time goes:
time: 141 us; the launch traced here: 140 us
  blocking collectives  70.7 us (50%)
  local copies, waits for them, and re-layouts  33.9 us (24%)
  matrix products  18.3 us (13%)
  other arithmetic  15.8 us (11%)
    all_gather x1, blocking collectives, shards(): every_list = lax.all_gather(picks[None, :, :, 1:], 'kv', axis=0, tiled=True)  23.3 us
    all_gather x1, blocking collectives, shards(): lax.all_gather(cmp_piece, 'kv', axis=1, tiled=True)  19.1 us
    all_gather x1, blocking collectives, shards(): lax.all_gather(export, 'kv', axis=0, tiled=True)  18.9 us
    all_gather x1, blocking collectives, shards(): lax.all_gather(mixed, 'tp', axis=1, tiled=True).astype(jnp.float32)  9.43 us
    dynamic_slice x16, local copies, waits for them, and re-layouts, shards(): lax.map(one_sequence, (queries, remote_entries, picks, sel_pairs, gates,...  8.72 us
    unnamed x24, local copies, waits for them, and re-layouts  8.52 us
    sub x8, other arithmetic, masked_weights(): expd = jnp.where(valid, jnp.exp(scores - top), 0.0)  7.55 us
    dot_general x5, matrix products, project(): jnp.dot(rows, weight_matrix, preferred_element_type=jnp.float32)  6.41 us

commit v1 on v0

--- a/solution.py
+++ b/solution.py
@@ -172,7 +172,7 @@
     mixed = mixed.reshape(seqs * span, local_heads * HEAD_DIM)
     out_width = width // lax.axis_size("tp")
     own_columns = lax.dynamic_slice_in_dim(w_out, column * out_width, out_width, 1)
-    piece_wide = lax.all_gather(mixed, "tp", axis=1, tiled=True).astype(jnp.float32)
+    piece_wide = jnp.concatenate(lax.all_gather(mixed, "tp"), axis=1).astype(jnp.float32)
     scaled_piece = (piece_wide * out_gain[None, :]).astype(jnp.bfloat16)
     total = jnp.dot(scaled_piece, own_columns, preferred_element_type=jnp.float32)
     squares = jnp.sum(piece_wide * piece_wide, axis=-1)

time: 141 us -> 142 us (level)
  no operation moved by 1% of the time
where the time goes in v1:
time: 142 us; the launch traced here: 141 us
  blocking collectives  70.7 us (50%)
  local copies, waits for them, and re-layouts  34.1 us (24%)
  matrix products  18.3 us (13%)
  other arithmetic  16.7 us (12%)
    all_gather x1, blocking collectives, shards(): every_list = lax.all_gather(picks[None, :, :, 1:], 'kv', axis=0, tiled=True)  23.3 us
    all_gather x1, blocking collectives, shards(): lax.all_gather(cmp_piece, 'kv', axis=1, tiled=True)  19.1 us
    all_gather x1, blocking collectives, shards(): lax.all_gather(export, 'kv', axis=0, tiled=True)  18.9 us
    all_gather x1, blocking collectives, shards(): lax.all_gather(mixed, 'tp')  9.43 us
    dynamic_slice x16, local copies, waits for them, and re-layouts, shards(): lax.map(one_sequence, (queries, remote_entries, picks, sel_pairs, gates,...  8.72 us
    unnamed x24, local copies, waits for them, and re-layouts  8.52 us
    sub x8, other arithmetic, masked_weights(): expd = jnp.where(valid, jnp.exp(scores - top), 0.0)  7.55 us
    dot_general x5, matrix products, project(): jnp.dot(rows, weight_matrix, preferred_element_type=jnp.float32)  6.41 us

profile of v1, /device:TPU:0, one launch (start us, length us, event | category | flops | bytes accessed | tf_op | source)
XLA Modules:
  0.0 140.9 jit_solution(8273780120586554388)
XLA Ops:
  0.2 1.3 copy.66
  2.6 23.3 %all-gather.1 = s32[64,2,15]{2,1,0:T(2,128)S(1)} all-gather(s32[4,2,15]{2,1,0:T(2,128)S(1)} %slice.87), channel_id=3, replica_groups=mesh['kv'=16,'tp'=2] {'kv'}, dimensions={0}, use_global_device_ids=true | all-gather | bytes 8160 | tf_op jit(solution)/shard_map/all_gather | solution.py:104
  25.9 1.2 compare_reduce_fusion
  28.2 18.9 %all-gather.2 = bf16[1024,2,128]{2,0,1:T(8,128)(2,1)S(1)} all-gather(bf16[64,2,128]{2,0,1:T(8,128)(2,1)S(1)} %get-tuple-element.167), channel_id=4, replica_groups=mesh['kv'=16,'tp'=2] {'kv'}, dimensions={0}, use_global_device_ids=true | all-gather | bytes 557056 | tf_op jit(solution)/shard_map/all_gather | solution.py:114
  47.2 1.0 copy.56
  48.2 1.8 %convolution_convert_fusion.2 = bf16[4,64,2,64]{1,3,2,0:T(8,128)(2,1)S(1)} fusion(bf16[2,64,2048,1]{2,1,0,3:T(8,128)(2,1)} %bitcast.234, bf16[4,64,2048]{2,1,0:T(8,128)(2,1)S(1)} %copy-done), kind=kOutput, calls=%fused_computation.69 | convolution fusion | flops 134250496 | bytes 1638400 | tf_op jit(solution)/shard_map/dot_general | solution.py:84
  51.1 1.2 copy.60
  54.3 19.1 %all-gather = bf16[4,64,2,128]{3,2,1,0:T(2,128)(2,1)S(1)} all-gather(bf16[4,4,2,128]{3,2,1,0:T(2,128)(2,1)S(1)} %pad_maximum_fusion.3), channel_id=2, replica_groups=mesh['kv'=16,'tp'=2] {'kv'}, dimensions={1}, use_global_device_ids=true | all-gather | bytes 139264 | tf_op jit(solution)/shard_map/all_gather | solution.py:115
  74.1 4.0 %copy.65 = bf16[2048,512]{0,1:T(8,128)(2,1)} copy(bf16[2048,512]{1,0:T(8,128)(2,1)} %param.18) | data formatting | bytes 4194304 | tf_op args[1]
  78.1 2.8 %fusion.53 = f32[4,64,8,64]{1,3,2,0:T(8,128)S(1)} fusion(bf16[8,64,2048,1]{2,1,0,3:T(8,128)(2,1)} %bitcast.229, bf16[4,64,2048]{2,1,0:T(8,128)(2,1)S(1)} %copy-done), kind=kOutput, calls=%fused_computation.76 | convolution fusion | flops 536870912 | bytes 3670016 | tf_op jit(solution)/shard_map/dot_general | solution.py:84
  83.1 43.9 %while.11 = (s32[]{:T(128)}, bf16[4,64,512]{2,1,0:T(8,128)(2,1)}, s32[4]{0:T(128)}, f32[4,64,2,8]{1,3,2,0:T(8,128)}, bf16[4,16,4,2,128]{4,2,1,3,0:T(4,128)(2,1)}...) while((s32[]{:T(128)}, bf16[4,64,512]{2,1,0:T(8,128)(2,1)}, ...), condition=%wide.region_8.9_spmd.clone, body=%wide.region_3.8_spmd.clone.sunk | while | flops 147700704 | bytes 25832684 | solution.py:171
  84.2 0.7 copy-done.1
  86.0 1.1 broadcast_in_dim.207
  87.1 1.8 %fusion.132 = (f32[2,4,64]{2,1,0:T(4,128)S(1)}, f32[2,4,64,1024]{3,2,1,0:T(8,128)S(1)}) fusion(f32[2,1024,64,4]{1,2,3,0:T(8,128)S(1)} %fusion.131, pred[2,64,1024]{2,1,0:T(8,128)(4,1)} %broadcast_in_dim.207), kind=kOutput, calls=%fused_computation.149.clone.1 | output fusion | flops 3146751 | bytes 4327424 | tf_op jit(solution)/shard_map/while/body/eval_jaxpr/sub | solution.py:33
  89.6 0.9 fusion.133
  90.5 0.9 constant_dynamic-slice_fusion.9
  95.2 0.7 copy-done.1
  97.0 1.1 broadcast_in_dim.207
  98.0 1.8 %fusion.132 = (f32[2,4,64]{2,1,0:T(4,128)S(1)}, f32[2,4,64,1024]{3,2,1,0:T(8,128)S(1)}) fusion(f32[2,1024,64,4]{1,2,3,0:T(8,128)S(1)} %fusion.131, pred[2,64,1024]{2,1,0:T(8,128)(4,1)} %broadcast_in_dim.207), kind=kOutput, calls=%fused_computation.149.clone.1 | output fusion | flops 3146751 | bytes 4327424 | tf_op jit(solution)/shard_map/while/body/eval_jaxpr/sub | solution.py:33
  100.6 0.9 fusion.133
  101.5 0.9 constant_dynamic-slice_fusion.9
  107.9 1.1 broadcast_in_dim.207
  109.0 1.8 %fusion.132 = (f32[2,4,64]{2,1,0:T(4,128)S(1)}, f32[2,4,64,1024]{3,2,1,0:T(8,128)S(1)}) fusion(f32[2,1024,64,4]{1,2,3,0:T(8,128)S(1)} %fusion.131, pred[2,64,1024]{2,1,0:T(8,128)(4,1)} %broadcast_in_dim.207), kind=kOutput, calls=%fused_computation.149.clone.1 | output fusion | flops 3146751 | bytes 4327424 | tf_op jit(solution)/shard_map/while/body/eval_jaxpr/sub | solution.py:33
  111.5 0.9 fusion.133
  112.5 0.9 constant_dynamic-slice_fusion.9
  118.9 1.1 broadcast_in_dim.207
  120.0 1.8 %fusion.132 = (f32[2,4,64]{2,1,0:T(4,128)S(1)}, f32[2,4,64,1024]{3,2,1,0:T(8,128)S(1)}) fusion(f32[2,1024,64,4]{1,2,3,0:T(8,128)S(1)} %fusion.131, pred[2,64,1024]{2,1,0:T(8,128)(4,1)} %broadcast_in_dim.207), kind=kOutput, calls=%fused_computation.149.clone.1 | output fusion | flops 3146751 | bytes 4327424 | tf_op jit(solution)/shard_map/while/body/eval_jaxpr/sub | solution.py:33
  122.5 0.9 fusion.133
  123.5 0.9 constant_dynamic-slice_fusion.9
  127.0 9.4 %all_gather.15 = bf16[2,256,512]{2,1,0:T(8,128)(2,1)S(1)} all-gather(bf16[1,256,512]{2,1,0:T(8,128)(2,1)} %bitcast.240), channel_id=1, replica_groups=mesh['kv'=16,'tp'=2] {'tp'}, dimensions={0}, use_global_device_ids=true | all-gather | bytes 786432 | tf_op jit(solution)/shard_map/all_gather | solution.py:175
  136.7 0.9 fusion.49
  137.8 3.1 %fusion.46 = bf16[256,1024]{1,0:T(8,128)(2,1)} fusion(bf16[256,1024]{0,1:T(8,128)(2,1)S(1)} %fusion.49, bf16[1024,2048]{1,0:T(8,128)(2,1)} %param.29, s32[]{:T(128)S(6)} %select_n.31, f32[256]{0:T(256)S(1)} %add_rsqrt_fusion), kind=kOutput, calls=%fused_computation.66 | convolution fusion | flops 537395200 | bytes 3146756 | tf_op jit(solution)/shard_map/dot_general | solution.py:177
  (233 shorter events, 31.6 us)
Async XLA Ops:
  0.0 1.5 %copy-start = (bf16[4,64,2048]{2,1,0:T(8,128)(2,1)S(1)}, bf16[4,64,2048]{2,1,0:T(8,128)(2,1)}, u32[]{:S(2)}) copy-start(bf16[4,64,2048]{2,1,0:T(8,128)(2,1)} %param.17) | copy-start | bytes 3145732
  0.0 2.5 %copy-start.14 = (s32[4,1,2,16]{3,2,1,0:T(2,128)S(1)}, s32[4,1,2,16]{3,2,1,0:T(2,128)}, u32[]{:S(2)}) copy-start(s32[4,1,2,16]{3,2,1,0:T(2,128)} %param.31) | copy-start | bytes 1540
  0.0 27.3 %copy-start.9 = (bf16[2048,128]{1,0:T(8,128)(2,1)S(1)}, bf16[2048,128]{1,0:T(8,128)(2,1)}, u32[]{:S(2)}) copy-start(bf16[2048,128]{1,0:T(8,128)(2,1)} %param.22) | copy-start | bytes 1572868
  25.9 21.3 %copy-start.10 = (bf16[2048,128]{1,0:T(8,128)(2,1)S(1)}, bf16[2048,128]{1,0:T(8,128)(2,1)}, u32[]{:S(2)}) copy-start(bf16[2048,128]{1,0:T(8,128)(2,1)} %param.19) | copy-start | bytes 1572868
  48.2 2.5 %copy-start.11 = (bf16[2048,128]{1,0:T(8,128)(2,1)S(1)}, bf16[2048,128]{1,0:T(8,128)(2,1)}, u32[]{:S(2)}) copy-start(bf16[2048,128]{1,0:T(8,128)(2,1)} %param.24) | copy-start | bytes 1572868
  48.2 2.5 %copy-start.15 = (bf16[128,64]{0,1:T(8,128)(2,1)S(1)}, bf16[128,64]{0,1:T(8,128)(2,1)}, u32[]{:S(2)}) copy-start(bf16[128,64]{0,1:T(8,128)(2,1)} %param.25) | copy-start | bytes 49156
  52.4 1.5 %copy-start.12 = (bf16[2048,128]{1,0:T(8,128)(2,1)S(1)}, bf16[2048,128]{1,0:T(8,128)(2,1)}, u32[]{:S(2)}) copy-start(bf16[2048,128]{1,0:T(8,128)(2,1)} %param.26) | copy-start | bytes 1572868
  52.4 1.5 %copy-start.16 = (bf16[128,64]{0,1:T(8,128)(2,1)S(1)}, bf16[128,64]{0,1:T(8,128)(2,1)}, u32[]{:S(2)}) copy-start(bf16[128,64]{0,1:T(8,128)(2,1)} %param.27) | copy-start | bytes 49156
  83.1 1.1 copy-start.3
  83.1 1.1 copy-start.5
  83.1 1.1 copy-start.7
  87.1 2.5 %copy-start.2 = (bf16[2,16,64,128]{3,2,1,0:T(8,128)(2,1)S(1)}, bf16[2,16,64,128]{3,2,1,0:T(8,128)(2,1)}, u32[]{:S(2)}) copy-start(bf16[2,16,64,128]{3,2,1,0:T(8,128)(2,1)} %copy-done.1) | copy-start | bytes 1572868 | tf_op jit(solution)/shard_map/while
  89.6 2.2 %copy-start.17 = (s32[4]{0:T(128)S(1)}, s32[4]{0:T(128)}, u32[]{:S(2)}) copy-start(s32[4]{0:T(128)} %get-tuple-element.302) | copy-start | bytes 52 | tf_op jit(solution)/shard_map/while
  90.5 3.6 %copy-start.4 = (bf16[16,64,2,128]{3,1,0,2:T(8,128)(2,1)S(1)}, bf16[16,64,2,128]{3,1,0,2:T(8,128)(2,1)}, u32[]{:S(2)}) copy-start(bf16[16,64,2,128]{3,1,0,2:T(8,128)(2,1)} %copy-done.3) | copy-start | bytes 1572868 | tf_op jit(solution)/shard_map/while
  90.5 3.6 %copy-start.6 = (bf16[4,64,8,64]{1,3,2,0:T(8,128)(2,1)S(1)}, bf16[4,64,8,64]{1,3,2,0:T(8,128)(2,1)}, u32[]{:S(2)}) copy-start(bf16[4,64,8,64]{1,3,2,0:T(8,128)(2,1)} %copy-done.5) | copy-start | bytes 786436 | tf_op jit(solution)/shard_map/while
  90.5 3.6 %copy-start.8 = (bf16[4,64,2,128]{3,1,2,0:T(8,128)(2,1)S(1)}, bf16[4,64,2,128]{3,1,2,0:T(8,128)(2,1)}, u32[]{:S(2)}) copy-start(bf16[4,64,2,128]{3,1,2,0:T(8,128)(2,1)} %copy-done.7) | copy-start | bytes 393220 | tf_op jit(solution)/shard_map/while
  94.1 1.1 copy-start.5
  98.0 2.5 %copy-start.2 = (bf16[2,16,64,128]{3,2,1,0:T(8,128)(2,1)S(1)}, bf16[2,16,64,128]{3,2,1,0:T(8,128)(2,1)}, u32[]{:S(2)}) copy-start(bf16[2,16,64,128]{3,2,1,0:T(8,128)(2,1)} %copy-done.1) | copy-start | bytes 1572868 | tf_op jit(solution)/shard_map/while
  100.6 2.2 %copy-start.17 = (s32[4]{0:T(128)S(1)}, s32[4]{0:T(128)}, u32[]{:S(2)}) copy-start(s32[4]{0:T(128)} %get-tuple-element.302) | copy-start | bytes 52 | tf_op jit(solution)/shard_map/while
  101.5 3.6 %copy-start.4 = (bf16[16,64,2,128]{3,1,0,2:T(8,128)(2,1)S(1)}, bf16[16,64,2,128]{3,1,0,2:T(8,128)(2,1)}, u32[]{:S(2)}) copy-start(bf16[16,64,2,128]{3,1,0,2:T(8,128)(2,1)} %copy-done.3) | copy-start | bytes 1572868 | tf_op jit(solution)/shard_map/while
  101.5 3.6 %copy-start.6 = (bf16[4,64,8,64]{1,3,2,0:T(8,128)(2,1)S(1)}, bf16[4,64,8,64]{1,3,2,0:T(8,128)(2,1)}, u32[]{:S(2)}) copy-start(bf16[4,64,8,64]{1,3,2,0:T(8,128)(2,1)} %copy-done.5) | copy-start | bytes 786436 | tf_op jit(solution)/shard_map/while
  101.5 3.6 %copy-start.8 = (bf16[4,64,2,128]{3,1,2,0:T(8,128)(2,1)S(1)}, bf16[4,64,2,128]{3,1,2,0:T(8,128)(2,1)}, u32[]{:S(2)}) copy-start(bf16[4,64,2,128]{3,1,2,0:T(8,128)(2,1)} %copy-done.7) | copy-start | bytes 393220 | tf_op jit(solution)/shard_map/while
  109.0 2.5 %copy-start.2 = (bf16[2,16,64,128]{3,2,1,0:T(8,128)(2,1)S(1)}, bf16[2,16,64,128]{3,2,1,0:T(8,128)(2,1)}, u32[]{:S(2)}) copy-start(bf16[2,16,64,128]{3,2,1,0:T(8,128)(2,1)} %copy-done.1) | copy-start | bytes 1572868 | tf_op jit(solution)/shard_map/while
  111.5 2.2 %copy-start.17 = (s32[4]{0:T(128)S(1)}, s32[4]{0:T(128)}, u32[]{:S(2)}) copy-start(s32[4]{0:T(128)} %get-tuple-element.302) | copy-start | bytes 52 | tf_op jit(solution)/shard_map/while
  112.5 3.6 %copy-start.4 = (bf16[16,64,2,128]{3,1,0,2:T(8,128)(2,1)S(1)}, bf16[16,64,2,128]{3,1,0,2:T(8,128)(2,1)}, u32[]{:S(2)}) copy-start(bf16[16,64,2,128]{3,1,0,2:T(8,128)(2,1)} %copy-done.3) | copy-start | bytes 1572868 | tf_op jit(solution)/shard_map/while
  112.5 3.6 %copy-start.6 = (bf16[4,64,8,64]{1,3,2,0:T(8,128)(2,1)S(1)}, bf16[4,64,8,64]{1,3,2,0:T(8,128)(2,1)}, u32[]{:S(2)}) copy-start(bf16[4,64,8,64]{1,3,2,0:T(8,128)(2,1)} %copy-done.5) | copy-start | bytes 786436 | tf_op jit(solution)/shard_map/while
  112.5 3.6 %copy-start.8 = (bf16[4,64,2,128]{3,1,2,0:T(8,128)(2,1)S(1)}, bf16[4,64,2,128]{3,1,2,0:T(8,128)(2,1)}, u32[]{:S(2)}) copy-start(bf16[4,64,2,128]{3,1,2,0:T(8,128)(2,1)} %copy-done.7) | copy-start | bytes 393220 | tf_op jit(solution)/shard_map/while
  120.0 2.5 %copy-start.2 = (bf16[2,16,64,128]{3,2,1,0:T(8,128)(2,1)S(1)}, bf16[2,16,64,128]{3,2,1,0:T(8,128)(2,1)}, u32[]{:S(2)}) copy-start(bf16[2,16,64,128]{3,2,1,0:T(8,128)(2,1)} %copy-done.1) | copy-start | bytes 1572868 | tf_op jit(solution)/shard_map/while
  122.5 2.2 %copy-start.17 = (s32[4]{0:T(128)S(1)}, s32[4]{0:T(128)}, u32[]{:S(2)}) copy-start(s32[4]{0:T(128)} %get-tuple-element.302) | copy-start | bytes 52 | tf_op jit(solution)/shard_map/while
  123.5 3.6 %copy-start.4 = (bf16[16,64,2,128]{3,1,0,2:T(8,128)(2,1)S(1)}, bf16[16,64,2,128]{3,1,0,2:T(8,128)(2,1)}, u32[]{:S(2)}) copy-start(bf16[16,64,2,128]{3,1,0,2:T(8,128)(2,1)} %copy-done.3) | copy-start | bytes 1572868 | tf_op jit(solution)/shard_map/while
  123.5 3.6 %copy-start.6 = (bf16[4,64,8,64]{1,3,2,0:T(8,128)(2,1)S(1)}, bf16[4,64,8,64]{1,3,2,0:T(8,128)(2,1)}, u32[]{:S(2)}) copy-start(bf16[4,64,8,64]{1,3,2,0:T(8,128)(2,1)} %copy-done.5) | copy-start | bytes 786436 | tf_op jit(solution)/shard_map/while
  123.5 3.6 %copy-start.8 = (bf16[4,64,2,128]{3,1,2,0:T(8,128)(2,1)S(1)}, bf16[4,64,2,128]{3,1,2,0:T(8,128)(2,1)}, u32[]{:S(2)}) copy-start(bf16[4,64,2,128]{3,1,2,0:T(8,128)(2,1)} %copy-done.7) | copy-start | bytes 393220 | tf_op jit(solution)/shard_map/while
  (13 other events, 12.5 us)
